TPU v7x, 32 devices: a whole 2x2x4 slice. The times are simulated.
32 devices in a mesh: ep: 8 (over z, x), tp: 4 (over y, core).
Axes of the slice: x: 2, y: 2, z: 4, core: 2. Of those that a mesh axis runs over, the one named last changes fastest.
Arguments:
- mix_query: bfloat16 [16384, 2048], P('ep', 'tp'), may hold values from -6 to 6
- mix_key: bfloat16 [16384, 2048], P('ep', 'tp'), may hold values from -6 to 6
- mix_value: bfloat16 [16384, 2048], P('ep', 'tp'), may hold values from -6 to 6
- mix_gate: bfloat16 [16384, 2048], P('ep', 'tp'), may hold values from -6 to 6
- log_decay: float32 [16384, 8], P('ep', 'tp'), may hold values from -1 to 0, as said below
- ret_gain: float32 [2048], P('tp'), may hold values from 0.1 to 1.9
- w_out: bfloat16 [2048, 2048], replicated, may hold values from -0.125 to 0.125
- moe_in: bfloat16 [1024, 2048], P(('ep', 'tp')), may hold values from -6 to 6
- route_ids: int32 [1024, 2], P(('ep', 'tp')), may hold values from 0 to 7, as said below
- route_weights: float32 [1024, 2], P(('ep', 'tp')), may hold values from 0.1 to 1
- moe_gain: float32 [2048], replicated, may hold values from 0.1 to 1.9
- w_gate: bfloat16 [8, 2048, 7168], P('ep', None, 'tp'), may hold values from -0.125 to 0.125
- w_up: bfloat16 [8, 2048, 7168], P('ep', None, 'tp'), may hold values from -0.125 to 0.125
- w_down: bfloat16 [8, 7168, 2048], P('ep', 'tp'), may hold values from -0.0625 to 0.0625
Outputs:
- mix_out: bfloat16 [16384, 2048], P(('ep', 'tp'))
- moe_out: bfloat16 [1024, 2048], P(('ep', 'tp'))
Inputs may be any that keep to these rules, and one draw needn't show every extreme that they name: `log_decay`: log of a decay. `route_ids`: each row names 2 different experts. Among the rows of one device no expert is named by more than 16 rows, and one expert is named by exactly 16 rows of every device.
All inputs are finite; a program needn't handle non-finite values.
Results may differ from a plain program's by a relative error of at most 0.015.
Values may be sent and summed in bfloat16 or wider, within the bound.
A program may use at most 128 MiB of HBM per device.

v0:
```python
import functools

import jax
import jax.numpy as jnp
import numpy as np
from jax import lax
from jax.experimental import pallas as pl
from jax.experimental.pallas import tpu as pltpu
from jax.sharding import PartitionSpec as P

HEAD_DIM = 256
BLOCK = 512
norm_eps = 1e-06
F32 = jnp.float32
BF16 = jnp.bfloat16
MESH = pl.DeviceIdType.MESH
VMEM_LIMIT = 67043328
COLS = 512


def dot(a, b, ca=1, cb=0):
    return lax.dot_general(a, b, (((ca,), (cb,)), ((), ())), preferred_element_type=F32)


def split3(x):
    a = x.astype(BF16)
    rest = x - a.astype(F32)
    b = rest.astype(BF16)
    c = (rest - b.astype(F32)).astype(BF16)
    return a, b, c


def loop(count, body):
    def step(i, carry):
        body(i)
        return carry

    lax.fori_loop(0, count, step, 0)


def slots_of(ids, capacity, count):
    tokens = ids.shape[1]
    row = lax.broadcasted_iota(jnp.int32, (count, tokens), 0)
    expert = row // capacity
    first = ids[0:1, :] == expert
    second = ids[1:2, :] == expert
    member = jnp.where(first | second, 1.0, 0.0)
    earlier = jnp.where(
        lax.broadcasted_iota(jnp.int32, (tokens, tokens), 0)
        < lax.broadcasted_iota(jnp.int32, (tokens, tokens), 1),
        1.0,
        0.0,
    ).astype(BF16)
    taken = dot(member.astype(BF16), earlier)
    slot = (row - expert * capacity).astype(F32)
    return jnp.where(taken == slot, member, 0.0), first


def layer_kernel(
    x_ref, ids_ref, rw_ref, mgain_ref, rgain_ref, logs_ref, cos_r, sin_r, cos_b, sin_b,
    q_hbm, k_hbm, v_hbm, g_hbm, wg_hbm, wu_hbm, wd_hbm, wo_hbm,
    mix_hbm, moe_hbm,
    q_v, k_v, v_v, g_v, wg_v, wu_v, wd_v, wo_v,
    disp, x_v, hid, ybuf, rbuf, ysend, yrecv, fin, ret, omoe,
    lg, cum, bef, local, state, states, dm, drecv, smsg, srecv, pout, inc, heads_v, obuf,
    ld, ldw, a_s, a_r, gy_s, gy_r, gc_s, gc_r, d_s, d_r, s1_s, s1_r, s2_s, s2_r,
    h_s, h_r, c2_s, c2_r, y2_s, y2_r, r_s, r_r, o_s,
):
    E = lax.axis_size("ep")
    L = lax.axis_size("tp")
    chips = L // 2
    e = lax.axis_index("ep")
    t = lax.axis_index("tp")
    y, c = t // 2, t % 2
    partner = 2 * y + 1 - c
    heads, rows, hd = q_v.shape
    half = hd // 2
    blocks = rows // BLOCK
    steps = heads * blocks
    R = rows // L
    width = heads * hd
    capacity = disp.shape[1]
    D = disp.shape[2]
    NT = D // COLS
    group = E * capacity

    def ahead(k):
        return lax.rem(e + k, E)

    def behind(k):
        return lax.rem(e - k + E, E)

    def chip_ahead(v):
        return lax.rem(y + v, chips)

    def chip_behind(v):
        return lax.rem(y - v + chips, chips)

    def remote(src, dst, ss, rs, dev):
        return pltpu.make_async_remote_copy(
            src_ref=src, dst_ref=dst, send_sem=ss, recv_sem=rs,
            device_id=dev, device_id_type=MESH,
        )

    def load_head(i, src, dst, h):
        return pltpu.make_async_copy(src.at[:, h * hd : (h + 1) * hd], dst.at[h], ld.at[i, h])

    def load_weight(i):
        pairs = ((wg_hbm.at[0], wg_v), (wu_hbm.at[0], wu_v), (wd_hbm.at[0], wd_v), (wo_hbm, wo_v))
        return pltpu.make_async_copy(pairs[i][0], pairs[i][1], ldw.at[i])

    def token(k):
        return remote(disp.at[ahead(k)], x_v.at[t, e], a_s.at[k], a_r.at[k], {"ep": ahead(k)})

    def across(v, k):
        p = behind(k)
        dev = {"tp": 2 * chip_ahead(v) + c}
        return remote(x_v.at[t, p], x_v.at[t, p], gy_s.at[v, k], gy_r.at[v, k], dev)

    def beside(v, k):
        p = behind(k)
        g = 2 * chip_behind(v) + c
        return remote(x_v.at[g, p], x_v.at[g, p], gc_s.at[v, k], gc_r.at[v, k], {"tp": partner})

    def decay(k):
        return remote(dm, drecv.at[e], d_s.at[k], d_r.at[k], {"ep": ahead(k)})

    def scatter(h, k):
        return remote(
            smsg.at[h, ahead(k)], srecv.at[h, e], s1_s.at[h, k], s1_r.at[h, k], {"ep": ahead(k)}
        )

    def spread(h, k):
        return remote(
            pout.at[h, ahead(k)], inc.at[h, e], s2_s.at[h, k], s2_r.at[h, k], {"ep": ahead(k)}
        )

    def lane_ahead(i):
        v, flip = i // 2, i % 2
        return 2 * chip_ahead(v) + c + flip * (1 - 2 * c)

    def head_copy(h, i):
        d = lane_ahead(i)
        return remote(
            g_v.at[h, pl.ds(pl.multiple_of(d * R, R), R)],
            heads_v.at[:, pl.ds(pl.multiple_of(t * width + h * hd, hd), hd)],
            h_s.at[h, i], h_r.at[h, i], {"tp": d},
        )

    def core_sum(n, yy):
        return remote(
            ybuf.at[n, 2 * yy + 1 - c], rbuf.at[n, yy], c2_s.at[n, yy], c2_r.at[n, yy],
            {"tp": partner},
        )

    def chip_sum(n, v):
        return remote(
            ysend.at[n, v - 1], yrecv.at[n, v - 1], y2_s.at[n, v], y2_r.at[n, v],
            {"tp": 2 * chip_ahead(v) + c},
        )

    def back(n, k):
        return remote(
            fin.at[n, ahead(k)], ret.at[n, e], r_s.at[n, k], r_r.at[n, k], {"ep": ahead(k)}
        )

    for h in range(heads):
        for i, (src, dst) in enumerate(((q_hbm, q_v), (k_hbm, k_v), (v_hbm, v_v))):
            load_head(i, src, dst, h).start()
    barrier = pltpu.get_barrier_semaphore()
    for k in range(1, E):
        pl.semaphore_signal(barrier, inc=1, device_id={"ep": ahead(k)}, device_id_type=MESH)
    for i in range(1, L):
        pl.semaphore_signal(barrier, inc=1, device_id={"tp": lane_ahead(i)}, device_id_type=MESH)

    floats = x_ref[...].astype(F32)
    scale = lax.rsqrt(jnp.mean(floats * floats, axis=-1, keepdims=True) + norm_eps)
    normed = (floats * scale * mgain_ref[...]).astype(BF16)
    chosen, first = slots_of(ids_ref[...], capacity, group)
    disp[...] = dot(chosen.astype(BF16), normed).astype(BF16).reshape(disp.shape)

    lg[...] = jnp.zeros_like(lg)
    for h in range(heads):
        for b in range(blocks):
            i = h * blocks + b
            lg[i : i + 1, :] = logs_ref[h : h + 1, b * BLOCK : (b + 1) * BLOCK]
    upper = jnp.where(
        lax.broadcasted_iota(jnp.int32, (BLOCK, BLOCK), 0)
        <= lax.broadcasted_iota(jnp.int32, (BLOCK, BLOCK), 1),
        1.0,
        0.0,
    ).astype(BF16)
    la, lb, lc = split3(lg[...])
    sums = dot(la, upper) + dot(lb, upper) + dot(lc, upper)
    cum[...] = sums
    lasts = sums[:, BLOCK - 1 : BLOCK]
    bef[...] = jnp.zeros_like(bef)
    dm[...] = jnp.zeros_like(dm)
    for h in range(heads):
        total = jnp.zeros((1, 1), F32)
        for b in range(blocks):
            i = h * blocks + b
            bef[i : i + 1, :] = jnp.exp(jnp.broadcast_to(total, (1, hd)))
            total = total + lasts[i : i + 1]
        dm[h : h + 1, :] = jnp.exp(jnp.broadcast_to(total, (1, hd)))

    pl.semaphore_wait(barrier, E - 1 + L - 1)
    for k in range(1, E):
        token(k).start()
    x_v[t, e] = disp[e]
    for v in range(1, chips):
        across(v, 0).start()
    beside(0, 0).start()
    for k in range(1, E):
        decay(k).start()
    drecv[e] = dm[...]
    load_weight(0).start()
    load_weight(1).start()
    for h in range(heads):
        load_head(3, g_hbm, g_v, h).start()
    load_weight(2).start()
    load_weight(3).start()

    per_step = -(-(E - 1) // max(steps - 1, 1))

    def pass_on(k):
        token(k).wait_recv()
        for v in range(1, chips):
            across(v, k).start()
        beside(0, k).start()

    def hand_over(k):
        for v in range(1, chips):
            across(v, k).wait_recv()
            beside(v, k).start()

    def prefix(h):
        if h == 0:
            for k in range(1, E):
                decay(k).wait_recv()
        for k in range(1, E):
            scatter(h, k).wait_recv()
        carry = jnp.zeros(srecv.shape[2:], F32)
        for p in range(E):
            pout[h, p] = carry.astype(BF16)
            carry = drecv[p, h : h + 1, :] * carry + srecv[h, p].astype(F32)
        for k in range(1, E):
            spread(h, k).start()
        inc[h, e] = pout[h, e]

    def retention(j):
        h, b = j // blocks, j % blocks

        @pl.when(b == 0)
        def _():
            state[...] = jnp.zeros_like(state)
            for hh in range(heads):

                @pl.when(h == hh)
                def _():
                    for i, (src, dst) in enumerate(((q_hbm, q_v), (k_hbm, k_v), (v_hbm, v_v))):
                        load_head(i, src, dst, hh).wait()

        at = pl.ds(pl.multiple_of(b * BLOCK, BLOCK), BLOCK)
        cum_row = cum[pl.ds(j, 1), :]
        cum_col = jnp.transpose(jnp.broadcast_to(cum_row, (8, BLOCK)))[:, 0:1]
        last = cum_row[:, BLOCK - 1 : BLOCK]
        cb, sb = cos_b[e * blocks + b], sin_b[e * blocks + b]
        cosine = cos_r[...] * cb - sin_r[...] * sb
        sine = sin_r[...] * cb + cos_r[...] * sb

        def rotate(x):
            front = x[:, :half].astype(F32)
            back_half = x[:, half:].astype(F32)
            return jnp.concatenate(
                [front * cosine - back_half * sine, back_half * cosine + front * sine], axis=1
            )

        q_rot = rotate(q_v[h, at, :]).astype(BF16)
        k_rot = (rotate(k_v[h, at, :]) * hd ** (-0.5)).astype(BF16)
        value = v_v[h, at, :]
        q_v[h, at, :] = (q_rot.astype(F32) * jnp.exp(cum_col)).astype(BF16)
        old = state[...]
        states[j] = old
        step = BLOCK // 2
        for i in range(2):
            r0, reach = i * step, (i + 1) * step
            scores = dot(q_rot[r0 : r0 + step], k_rot[:reach], 1, 1)
            causal = (
                lax.broadcasted_iota(jnp.int32, (step, reach), 0) + r0
                >= lax.broadcasted_iota(jnp.int32, (step, reach), 1)
            )
            gap = cum_col[r0 : r0 + step] - cum_row[:, :reach]
            mask = jnp.exp(jnp.where(causal, gap, -1e30))
            weights = (scores * mask).astype(BF16)
            local[j, r0 : r0 + step, :] = dot(weights, value[:reach])
        k_decayed = (k_rot.astype(F32) * jnp.exp(last - cum_col)).astype(BF16)
        fresh = jnp.exp(last) * old + dot(k_decayed, value, 0, 0)
        state[...] = fresh

        for hh in range(heads):

            @pl.when(j == (hh + 1) * blocks - 1)
            def _():
                smsg[hh] = fresh.astype(BF16).reshape(smsg.shape[1:])
                for k in range(1, E):
                    scatter(hh, k).start()
                srecv[hh, e] = smsg[hh, e]

        for i in range(per_step):
            k = 1 + j * per_step + i

            @pl.when(k < E)
            def _():
                pass_on(k)

        for i in range(per_step):
            k = 1 + (j - 1) * per_step + i

            @pl.when((j > 0) & (k < E))
            def _():
                hand_over(k)

        @pl.when(j == 0)
        def _():
            hand_over(0)

        for hh in range(heads - 1):

            @pl.when(j == (hh + 1) * blocks + 2)
            def _():
                prefix(hh)

    loop(steps, retention)
    for i in range(per_step):
        k = 1 + (steps - 1) * per_step + i
        if k < E:
            hand_over(k)

    def finish(h):
        for k in range(1, E):
            spread(h, k).wait_recv()
        load_head(3, g_hbm, g_v, h).wait()
        incoming = inc[h].astype(F32).reshape(hd, hd)
        gain = rgain_ref[:, h * hd : (h + 1) * hd]

        def piece(n):
            i = lax.rem(n + 2, L)
            d = lane_ahead(i)
            j = h * blocks + d * R // BLOCK
            at = pl.ds(pl.multiple_of(d * R, R), R)
            inner = pl.ds(pl.multiple_of(lax.rem(d * R, BLOCK), R), R)
            start = bef[pl.ds(j, 1), :] * incoming + states[j]
            retained = local[j, inner, :] + dot(q_v[h, at, :], start.astype(BF16))
            scale = lax.rsqrt(jnp.mean(retained * retained, axis=-1, keepdims=True) + norm_eps)
            gate = g_v[h, at, :].astype(F32)
            gate = gate / (1.0 + jnp.exp(-gate))
            out = (gate * retained * scale * gain).astype(BF16)
            g_v[h, at, :] = out

            @pl.when(i != 0)
            def _():
                head_copy(h, i).start()

            @pl.when(i == 0)
            def _():
                heads_v[:, pl.ds(pl.multiple_of(t * width + h * hd, hd), hd)] = out

        loop(L, piece)

    for v in range(chips):
        for k in range(E):
            beside(v, k).wait_recv()
    load_weight(0).wait()
    load_weight(1).wait()
    hidden_width = hid.shape[1]
    tile = 256 if hidden_width % 256 == 0 else 128

    def up(n):
        for h in range(heads):

            @pl.when(n == 5 - 4 * (heads - 1 - h))
            def _():
                finish(h)

        @pl.when(n == 2)
        def _():
            prefix(heads - 1)

        at = pl.ds(pl.multiple_of(n * tile, tile), tile)
        x = x_v[...].reshape(L * group, D)
        gate = dot(x, wg_v[:, at])
        rise = dot(x, wu_v[:, at])
        hid[:, at] = (gate / (1.0 + jnp.exp(-gate)) * rise).astype(BF16)

    loop(hidden_width // tile, up)

    load_weight(2).wait()

    def share(n):
        for yy in range(chips):
            core_sum(n, yy).wait_recv()
        for v in range(1, chips):
            yy = chip_ahead(v)
            total = ybuf[n, 2 * yy + c].astype(F32) + rbuf[n, yy].astype(F32)
            ysend[n, v - 1] = total.astype(BF16)
            chip_sum(n, v).start()

    def down(n):
        at = pl.ds(pl.multiple_of(n * COLS, COLS), COLS)
        ybuf[n] = dot(hid[...], wd_v[:, at]).astype(BF16).reshape(ybuf.shape[1:])
        for yy in range(chips):
            core_sum(n, yy).start()

        @pl.when(n > 0)
        def _():
            share(n - 1)

    loop(NT, down)
    share(NT - 1)

    load_weight(3).wait()
    for h in range(heads):
        for i in range(1, L):
            head_copy(h, i).wait_recv()

    def out_copy(n):
        at = pl.ds(pl.multiple_of(n * COLS, COLS), COLS)
        return pltpu.make_async_copy(obuf.at[n], mix_hbm.at[:, at], o_s.at[n])

    def project(n):
        at = pl.ds(pl.multiple_of(n * COLS, COLS), COLS)
        obuf[n] = dot(heads_v[...], wo_v[:, at]).astype(BF16)
        out_copy(n).start()
        total = ybuf[n, t].astype(F32) + rbuf[n, y].astype(F32)
        for v in range(1, chips):
            chip_sum(n, v).wait_recv()
            total = total + yrecv[n, v - 1].astype(F32)
        fin[n] = total.astype(BF16).reshape(fin.shape[1:])
        for k in range(1, E):
            back(n, k).start()
        ret[n, e] = fin[n, e]

    loop(NT, project)

    weight = chosen * jnp.where(first, rw_ref[0:1, :], rw_ref[1:2, :])
    terms = split3(weight)
    for n in range(NT):
        for k in range(1, E):
            back(n, k).wait_recv()
        got = ret[n].reshape(group, COLS)
        total = dot(terms[0], got, 0, 0) + dot(terms[1], got, 0, 0) + dot(terms[2], got, 0, 0)
        omoe[:, n * COLS : (n + 1) * COLS] = total.astype(BF16)
    moe_copy = pltpu.make_async_copy(omoe, moe_hbm, o_s.at[NT])
    moe_copy.start()

    for k in range(1, E):
        token(k).wait_send()
        decay(k).wait_send()
        for h in range(heads):
            scatter(h, k).wait_send()
            spread(h, k).wait_send()
        for n in range(NT):
            back(n, k).wait_send()
    for k in range(E):
        for v in range(1, chips):
            across(v, k).wait_send()
        for v in range(chips):
            beside(v, k).wait_send()
    for h in range(heads):
        for i in range(1, L):
            head_copy(h, i).wait_send()
    for n in range(NT):
        for yy in range(chips):
            core_sum(n, yy).wait_send()
        for v in range(1, chips):
            chip_sum(n, v).wait_send()
        out_copy(n).wait()
    moe_copy.wait()


def on_device(
    mix_query, mix_key, mix_value, mix_gate, log_decay, ret_gain, w_out,
    moe_in, route_ids, route_weights, moe_gain, w_gate, w_up, w_down,
):
    E = lax.axis_size("ep")
    L = lax.axis_size("tp")
    chips = L // 2
    rows, width = mix_query.shape
    heads = width // HEAD_DIM
    blocks = rows // BLOCK
    steps = heads * blocks
    half = HEAD_DIM // 2
    tokens, D = moe_in.shape
    capacity = 4 * tokens // E
    group = E * capacity
    hidden = w_gate.shape[2]
    NT = D // COLS
    R = rows // L
    part = HEAD_DIM // E
    inverse = 10000.0 ** (-(np.arange(half) * 2.0) / HEAD_DIM)
    fine = np.arange(BLOCK)[:, None] * inverse[None, :]
    coarse = (np.arange(E * blocks) * BLOCK)[:, None, None] * inverse[None, None, :]
    tables = [np.asarray(f(x), np.float32) for x in (fine, coarse) for f in (np.cos, np.sin)]
    vm = pl.BlockSpec(memory_space=pltpu.VMEM)
    hbm = pl.BlockSpec(memory_space=pl.ANY)
    pad = -(-steps // 8) * 8
    V = pltpu.VMEM
    S = pltpu.SemaphoreType.DMA
    return pl.pallas_call(
        layer_kernel,
        in_specs=[vm] * 10 + [hbm] * 8,
        out_specs=[hbm, hbm],
        out_shape=[
            jax.ShapeDtypeStruct((R, D), BF16),
            jax.ShapeDtypeStruct((tokens, D), BF16),
        ],
        scratch_shapes=[
            V((heads, rows, HEAD_DIM), BF16), V((heads, rows, HEAD_DIM), BF16),
            V((heads, rows, HEAD_DIM), BF16), V((heads, rows, HEAD_DIM), BF16),
            V((D, hidden), BF16), V((D, hidden), BF16), V((hidden, D), BF16), V(w_out.shape, BF16),
            V((E, capacity, D), BF16), V((L, E, capacity, D), BF16), V((L * group, hidden), BF16),
            V((NT, L, group, COLS), BF16), V((NT, chips, group, COLS), BF16),
            V((NT, chips - 1, group, COLS), BF16), V((NT, chips - 1, group, COLS), BF16),
            V((NT, E, capacity, COLS), BF16), V((NT, E, capacity, COLS), BF16),
            V((tokens, D), BF16),
            V((pad, BLOCK), F32), V((pad, BLOCK), F32), V((pad, HEAD_DIM), F32),
            V((steps, BLOCK, HEAD_DIM), F32), V((HEAD_DIM, HEAD_DIM), F32),
            V((steps, HEAD_DIM, HEAD_DIM), F32),
            V((8, HEAD_DIM), F32), V((E, 8, HEAD_DIM), F32),
            V((heads, E, part, HEAD_DIM), BF16), V((heads, E, part, HEAD_DIM), BF16),
            V((heads, E, part, HEAD_DIM), BF16), V((heads, E, part, HEAD_DIM), BF16),
            V((R, D), BF16), V((NT, R, COLS), BF16),
            S((4, heads)), S((4,)), S((E,)), S((E,)),
            S((chips, E)), S((chips, E)), S((chips, E)), S((chips, E)),
            S((E,)), S((E,)), S((heads, E)), S((heads, E)), S((heads, E)), S((heads, E)),
            S((heads, L)), S((heads, L)), S((NT, chips)), S((NT, chips)),
            S((NT, chips)), S((NT, chips)), S((NT, E)), S((NT, E)), S((NT + 1,)),
        ],
        compiler_params=pltpu.CompilerParams(
            collective_id=0, has_side_effects=True, vmem_limit_bytes=VMEM_LIMIT
        ),
        name="layer",
    )(
        moe_in, route_ids.T, route_weights.T, moe_gain.reshape(1, -1), ret_gain.reshape(1, -1),
        log_decay.T, *tables,
        mix_query, mix_key, mix_value, mix_gate, w_gate, w_up, w_down, w_out,
    )


def solution(mesh):
    in_specs = (
        P("ep", "tp"),
        P("ep", "tp"),
        P("ep", "tp"),
        P("ep", "tp"),
        P("ep", "tp"),
        P("tp"),
        P(),
        P(("ep", "tp"), None),
        P(("ep", "tp"), None),
        P(("ep", "tp"), None),
        P(),
        P("ep", None, "tp"),
        P("ep", None, "tp"),
        P("ep", "tp", None),
    )
    out_specs = (P(("ep", "tp"), None), P(("ep", "tp"), None))
    return jax.shard_map(
        lambda *args: tuple(on_device(*args)), mesh=mesh, in_specs=in_specs, out_specs=out_specs,
        check_vma=False,
    )
```

profile of v0, /device:TPU:0, one launch (start us, length us, event | category | flops | bytes accessed | tf_op | source)
XLA Modules:
  0.0 82.3 jit_solution(5410339542942133800)
XLA Ops:
  0.6 77.8 %layer.1 = (bf16[512,2048]{1,0:T(8,128)(2,1)}, bf16[32,2048]{1,0:T(8,128)(2,1)}) custom-call(bf16[32,2048]{1,0:T(8,128)(2,1)} %x_ref.1, s32[2,32]{1,0:T(2,128)} %bitcast.8, f32[2,32]{1,0:T(2,128)} %bitcast.9, f32[1,2048]{1,0:T(1,128)} %bitcast.6, f32[1,512]{1,0:T(1,128)} %bitcast.7, f32[2,2048]{1,0:T(2,128)} %bitcast.5, f32[512,128]{1,0:T(8,128)} %constant.8.clone.cos_r, ...), custom_call_target="tpu_custom_call" | custom-call | tf_op jit(solution)/shard_map/layer/pallas_call | solution.py:510
  78.4 0.0 copy-start
  78.4 3.2 %copy.22 = bf16[512,2048]{1,0:T(8,128)(2,1)} copy(bf16[512,2048]{1,0:T(8,128)(2,1)} %get-tuple-element.4) | data formatting | bytes 4194304
  81.6 0.0 copy-done
  81.6 0.7 copy.23
Async XLA Ops:
  78.4 3.2 %copy-start = (bf16[32,2048]{1,0:T(8,128)(2,1)S(1)}, bf16[32,2048]{1,0:T(8,128)(2,1)}, u32[]{:S(2)}) copy-start(bf16[32,2048]{1,0:T(8,128)(2,1)} %get-tuple-element.5) | copy-start | bytes 393220
where the time goes:
time: 82.4 us; the launch traced here: 82.3 us
  Pallas kernels  77.8 us (94%)
  local copies, waits for them, and re-layouts  3.85 us (5%)
    pallas_call x1, Pallas kernels, on_device(): pl.pallas_call(layer_kernel, in_specs=[vm] * 10 + [hbm] * 8, out_specs=[h...  77.8 us
    unnamed x4, local copies, waits for them, and re-layouts  3.85 us

commit v1 on v0

v1 whole, which is shorter than its diff:
```python
import functools

import jax
import jax.numpy as jnp
import numpy as np
from jax import lax
from jax.experimental import pallas as pl
from jax.experimental.pallas import tpu as pltpu
from jax.sharding import PartitionSpec as P

HEAD_DIM = 256
BLOCK = 512
norm_eps = 1e-06
F32 = jnp.float32
BF16 = jnp.bfloat16
MESH = pl.DeviceIdType.MESH
VMEM_LIMIT = 63000000
COLS = 512


def dot(a, b, ca=1, cb=0):
    return lax.dot_general(a, b, (((ca,), (cb,)), ((), ())), preferred_element_type=F32)


def split3(x):
    a = x.astype(BF16)
    rest = x - a.astype(F32)
    b = rest.astype(BF16)
    c = (rest - b.astype(F32)).astype(BF16)
    return a, b, c


def loop(count, body):
    def step(i, carry):
        body(i)
        return carry

    lax.fori_loop(0, count, step, 0)


def slots_of(ids, capacity, count):
    tokens = ids.shape[1]
    row = lax.broadcasted_iota(jnp.int32, (count, tokens), 0)
    expert = row // capacity
    first = ids[0:1, :] == expert
    second = ids[1:2, :] == expert
    member = jnp.where(first | second, 1.0, 0.0)
    earlier = jnp.where(
        lax.broadcasted_iota(jnp.int32, (tokens, tokens), 0)
        < lax.broadcasted_iota(jnp.int32, (tokens, tokens), 1),
        1.0,
        0.0,
    ).astype(BF16)
    taken = dot(member.astype(BF16), earlier)
    slot = (row - expert * capacity).astype(F32)
    return jnp.where(taken == slot, member, 0.0), first


def layer_kernel(
    x_hbm, ids_hbm, rw_hbm, mgain_hbm, rgain_hbm, logs_hbm, cosr_hbm, sinr_hbm, cosb_hbm, sinb_hbm,
    q_hbm, k_hbm, v_hbm, g_hbm, wg_hbm, wu_hbm, wd_hbm, wo_hbm,
    obuf, omoe,
    x_ref, ids_ref, rw_ref, mgain_ref, rgain_ref, logs_ref, cos_r, sin_r, cos_b, sin_b,
    q_v, k_v, v_v, g_v, wg_v, wu_v, wd_v, wo_v,
    disp, x_v, hid, ybuf, rbuf, ysend, yrecv, fin, ret,
    lg, cum, bef, local, state, states, dm, drecv, smsg, srecv, tsend, trecv, pout, inc, heads_v, hlast,
    lds, ld, ldw, a_s, a_r, gy_s, gy_r, gc_s, gc_r, d_s, d_r, s1_s, s1_r, t_s, t_r, s2_s, s2_r,
    h_s, h_r, c2_s, c2_r, y2_s, y2_r, r_s, r_r,
):
    E = lax.axis_size("ep")
    L = lax.axis_size("tp")
    chips = L // 2
    e = lax.axis_index("ep")
    t = lax.axis_index("tp")
    y, c = t // 2, t % 2
    partner = 2 * y + 1 - c
    heads, rows, hd = q_v.shape
    half = hd // 2
    blocks = rows // BLOCK
    steps = heads * blocks
    R = rows // L
    width = heads * hd
    capacity = disp.shape[1]
    D = disp.shape[2]
    NT = D // COLS
    group = E * capacity

    def ahead(k):
        return lax.rem(e + k, E)

    G = E // 2
    upper_half, place = e // G, e % G

    def flip(k):
        out, bit = 0, 1
        while bit < E:
            out = out + bit * ((e // bit + k // bit) % 2)
            bit *= 2
        return out

    def member(k):
        return upper_half * G + lax.rem(place + k, G)

    def chip_ahead(v):
        return lax.rem(y + v, chips)

    def chip_behind(v):
        return lax.rem(y - v + chips, chips)

    def remote(src, dst, ss, rs, dev):
        return pltpu.make_async_remote_copy(
            src_ref=src, dst_ref=dst, send_sem=ss, recv_sem=rs,
            device_id=dev, device_id_type=MESH,
        )

    def load_head(i, src, dst, h):
        return pltpu.make_async_copy(src.at[:, h * hd : (h + 1) * hd], dst.at[h], ld.at[i, h])

    def load_weight(i):
        pairs = ((wg_hbm.at[0], wg_v), (wu_hbm.at[0], wu_v), (wd_hbm.at[0], wd_v), (wo_hbm, wo_v))
        return pltpu.make_async_copy(pairs[i][0], pairs[i][1], ldw.at[i])

    def token(k):
        return remote(disp.at[flip(k)], x_v.at[t, e], a_s, a_r.at[k], {"ep": flip(k)})

    def across(v, k):
        p = flip(k)
        dev = {"tp": 2 * chip_ahead(v) + c}
        return remote(x_v.at[t, p], x_v.at[t, p], gy_s, gy_r.at[v - 1, k], dev)

    def beside(v, k):
        p = flip(k)
        g = 2 * chip_behind(v) + c
        return remote(x_v.at[g, p], x_v.at[g, p], gc_s, gc_r, {"tp": partner})

    def decay(k):
        return remote(dm, drecv.at[place], d_s, d_r, {"ep": member(k)})

    def scatter(h, k):
        return remote(
            smsg.at[h, lax.rem(place + k, G)], srecv.at[h, place], s1_s.at[h], s1_r.at[h],
            {"ep": member(k)},
        )

    def lift(h):
        return remote(tsend.at[h], trecv.at[h], t_s, t_r.at[h], {"ep": lax.rem(e + G, E)})

    def spread(h, k):
        return remote(
            pout.at[h, lax.rem(place + k, G)], inc.at[h, place], s2_s.at[h], s2_r.at[h],
            {"ep": member(k)},
        )

    def lane_ahead(i):
        v, flip = i // 2, i % 2
        return 2 * chip_ahead(v) + c + flip * (1 - 2 * c)

    def last_copy():
        d = lane_ahead(L - 1)
        return remote(
            g_v.at[heads - 1, pl.ds(pl.multiple_of(d * R, R), R)], hlast,
            h_s.at[heads - 1], h_r.at[1], {"tp": d},
        )

    last_source = 2 * chip_behind(chips - 1) + 1 - c
    last_rows = pl.ds(pl.multiple_of(last_source * width + (heads - 1) * hd, hd), hd)

    def head_copy(h, i):
        d = lane_ahead(i)
        return remote(
            g_v.at[h, pl.ds(pl.multiple_of(d * R, R), R)],
            heads_v.at[:, pl.ds(pl.multiple_of(t * width + h * hd, hd), hd)],
            h_s.at[h], h_r.at[0], {"tp": d},
        )

    def core_sum(n, yy):
        return remote(
            ybuf.at[n, 2 * yy + 1 - c], rbuf.at[n, yy], c2_s, c2_r.at[n],
            {"tp": partner},
        )

    def chip_sum(n, v):
        return remote(
            ysend.at[n, v - 1], yrecv.at[n, v - 1], y2_s, y2_r.at[n],
            {"tp": 2 * chip_ahead(v) + c},
        )

    def back(n, k):
        return remote(
            fin.at[n, ahead(k)], ret.at[n, e], r_s.at[n], r_r.at[n], {"ep": ahead(k)}
        )

    barrier = pltpu.get_barrier_semaphore()
    for k in range(1, E):
        pl.semaphore_signal(barrier, inc=1, device_id={"ep": flip(k)}, device_id_type=MESH)
    for i in range(1, L):
        pl.semaphore_signal(barrier, inc=1, device_id={"tp": lane_ahead(i)}, device_id_type=MESH)

    def done(ref, sem):
        pltpu.make_async_copy(ref, ref, sem).wait()

    small = [
        pltpu.make_async_copy(src, dst, lds.at[i])
        for i, (src, dst) in enumerate(
            (
                (x_hbm, x_ref), (mgain_hbm, mgain_ref), (ids_hbm, ids_ref), (logs_hbm, logs_ref),
                (cosr_hbm, cos_r), (sinr_hbm, sin_r), (cosb_hbm, cos_b), (sinb_hbm, sin_b),
                (rgain_hbm, rgain_ref), (rw_hbm, rw_ref),
            )
        )
    ]
    for copy in small:
        copy.start()
    for copy in small[:3]:
        copy.wait()
    for h in range(heads):
        for i, (src, dst) in ((1, (k_hbm, k_v)), (2, (v_hbm, v_v))):
            load_head(i, src, dst, h).start()
    for h in range(heads):
        load_head(0, q_hbm, q_v, h).start()

    floats = x_ref[...].astype(F32)
    scale = lax.rsqrt(jnp.mean(floats * floats, axis=-1, keepdims=True) + norm_eps)
    normed = (floats * scale * mgain_ref[...]).astype(BF16)
    chosen, first = slots_of(ids_ref[...], capacity, group)
    disp[...] = dot(chosen.astype(BF16), normed).astype(BF16).reshape(disp.shape)

    for copy in small[3:]:
        copy.wait()
    lg[...] = jnp.zeros_like(lg)
    for h in range(heads):
        for b in range(blocks):
            i = h * blocks + b
            lg[i : i + 1, :] = logs_ref[h : h + 1, b * BLOCK : (b + 1) * BLOCK]
    upper = jnp.where(
        lax.broadcasted_iota(jnp.int32, (BLOCK, BLOCK), 0)
        <= lax.broadcasted_iota(jnp.int32, (BLOCK, BLOCK), 1),
        1.0,
        0.0,
    ).astype(BF16)
    la, lb, lc = split3(lg[...])
    sums = dot(la, upper) + dot(lb, upper) + dot(lc, upper)
    cum[...] = sums
    lasts = sums[:, BLOCK - 1 : BLOCK]
    bef[...] = jnp.zeros_like(bef)
    dm[...] = jnp.zeros_like(dm)
    for h in range(heads):
        total = jnp.zeros((1, 1), F32)
        for b in range(blocks):
            i = h * blocks + b
            bef[i : i + 1, :] = jnp.exp(jnp.broadcast_to(total, (1, hd)))
            total = total + lasts[i : i + 1]
        dm[h : h + 1, :] = jnp.exp(jnp.broadcast_to(total, (1, hd)))

    pl.semaphore_wait(barrier, E - 1 + L - 1)
    mids = list(range(E - E // 4, E)) + list(range(E // 2, E - E // 4))
    near = list(range(2, E // 2))
    n4 = len(mids) // 4
    waves = [
        [1] + near[:1] + mids[:n4],
        mids[n4 : 2 * n4],
        near[1:],
        mids[2 * n4 :],
    ]
    order = [0] + waves[0] + waves[1] + waves[2] + waves[3]

    held = len(waves[3])

    def send_wave(i):
        for k in waves[i]:
            token(k).start()

    def pass_on(k):
        token(k).wait_recv()
        for v in range(1, chips):
            across(v, k).start()
        beside(0, k).start()

    def hand_over(k):
        for v in range(1, chips):
            across(v, k).wait_recv()
            beside(v, k).start()

    send_wave(0)
    x_v[t, e] = disp[e]
    for v in range(1, chips):
        across(v, 0).start()
    beside(0, 0).start()
    for k in range(1, G):
        decay(k).start()
    drecv[place] = dm[...]

    def tables_of(b):
        cb, sb = cos_b[e * blocks + b], sin_b[e * blocks + b]
        return cos_r[...] * cb - sin_r[...] * sb, sin_r[...] * cb + cos_r[...] * sb

    def rotate(x, cosine, sine):
        front = x[:, :half].astype(F32)
        rest = x[:, half:].astype(F32)
        return jnp.concatenate([front * cosine - rest * sine, rest * cosine + front * sine], axis=1)

    def column(row):
        return jnp.transpose(jnp.broadcast_to(row, (8, BLOCK)))[:, 0:1]

    def rows_of(b):
        return pl.ds(pl.multiple_of(b * BLOCK, BLOCK), BLOCK)

    for h in range(heads):
        load_head(1, k_hbm, k_v, h).wait()
        load_head(2, v_hbm, v_v, h).wait()
        state[...] = jnp.zeros_like(state)

        def update(b):
            j = h * blocks + b
            at = rows_of(b)
            cum_row = cum[pl.ds(j, 1), :]
            last = cum_row[:, BLOCK - 1 : BLOCK]
            k_rot = (rotate(k_v[h, at, :], *tables_of(b)) * hd ** (-0.5)).astype(BF16)
            k_v[h, at, :] = k_rot
            k_decayed = (k_rot.astype(F32) * jnp.exp(last - column(cum_row))).astype(BF16)
            old = state[...]
            states[j] = old
            state[...] = jnp.exp(last) * old + dot(k_decayed, v_v[h, at, :], 0, 0)
            if h == heads - 1:
                for k, step in ((order[1], 1), (order[2], blocks - 1)):

                    @pl.when(b == step)
                    def _():
                        pass_on(k)

        loop(blocks, update)
        smsg[h] = state[...].astype(BF16).reshape(smsg.shape[1:])
        for k in range(1, G):
            scatter(h, k).start()
        srecv[h, place] = smsg[h, place]
        if h == 0:
            send_wave(1)
    load_weight(0).start()
    load_weight(1).start()
    for h in range(heads):
        load_head(3, g_hbm, g_v, h).start()
    load_weight(2).start()
    load_weight(3).start()

    def scan(h, carry):
        for p in range(G):
            pout[h, p] = carry.astype(BF16)
            carry = drecv[p, h : h + 1, :] * carry + srecv[h, p].astype(F32)
        for k in range(1, G):
            spread(h, k).start()
        inc[h, place] = pout[h, place]
        return carry

    def arrivals(h):
        if h == 0:
            done(drecv.at[0 : G - 1], d_r)
        done(srecv.at[h, 0 : G - 1], s1_r.at[h])

    def prefix_low(h):
        @pl.when(upper_half == 0)
        def _():
            arrivals(h)
            carry = scan(h, jnp.zeros(srecv.shape[2:], F32))
            tsend[h] = carry.astype(BF16)
            lift(h).start()

    def prefix_high(h):
        @pl.when(upper_half == 1)
        def _():
            arrivals(h)
            lift(h).wait_recv()
            scan(h, trecv[h].astype(F32))

    def within(j):
        h, b = j // blocks, j % blocks
        for hh in range(heads):

            @pl.when(j == hh * blocks)
            def _():
                load_head(0, q_hbm, q_v, hh).wait()

        at = rows_of(b)
        cum_row = cum[pl.ds(j, 1), :]
        cum_col = column(cum_row)
        q_rot = rotate(q_v[h, at, :], *tables_of(b)).astype(BF16)
        k_rot = k_v[h, at, :]
        value = v_v[h, at, :]
        q_v[h, at, :] = (q_rot.astype(F32) * jnp.exp(cum_col)).astype(BF16)
        step = BLOCK // 2
        for i in range(2):
            r0, reach = i * step, (i + 1) * step
            scores = dot(q_rot[r0 : r0 + step], k_rot[:reach], 1, 1)
            causal = (
                lax.broadcasted_iota(jnp.int32, (step, reach), 0) + r0
                >= lax.broadcasted_iota(jnp.int32, (step, reach), 1)
            )
            gap = cum_col[r0 : r0 + step] - cum_row[:, :reach]
            mask = jnp.exp(jnp.where(causal, gap, -1e30))
            weights = (scores * mask).astype(BF16)
            local[j, r0 : r0 + step, :] = dot(weights, value[:reach])

        for i, k in enumerate(order[3:-held]):

            @pl.when(j == min(1 + 2 * i + i // 2, steps - 1))
            def _():
                pass_on(k)

        for i, k in enumerate(order[:2]):

            @pl.when(j == steps // 2 + min(2 * i, steps // 2 - 1))
            def _():
                hand_over(k)

        for hh in range(heads):
            if high_step(hh) < steps:

                @pl.when(j == high_step(hh))
                def _():
                    prefix_high(hh)

            @pl.when(j == low_step(hh))
            def _():
                prefix_low(hh)
                if hh == 0:
                    send_wave(2)
                if hh == heads - 1:
                    send_wave(3)

    def low_step(h):
        return min(max(0, 3 - 3 * (heads - 1 - h)), steps - 1)

    def high_step(h):
        return low_step(h) + 4

    loop(steps, within)
    for h in range(heads):
        if high_step(h) >= steps:
            prefix_high(h)

    def finish(h):
        done(inc.at[h, 0 : G - 1], s2_r.at[h])
        load_head(3, g_hbm, g_v, h).wait()
        incoming = inc[h].astype(F32).reshape(hd, hd)
        gain = rgain_ref[:, h * hd : (h + 1) * hd]

        def piece(n):
            i = lax.rem(n + 2, L)
            d = lane_ahead(i)
            j = h * blocks + d * R // BLOCK
            at = pl.ds(pl.multiple_of(d * R, R), R)
            inner = pl.ds(pl.multiple_of(lax.rem(d * R, BLOCK), R), R)
            start = bef[pl.ds(j, 1), :] * incoming + states[j]
            retained = local[j, inner, :] + dot(q_v[h, at, :], start.astype(BF16))
            scale = lax.rsqrt(jnp.mean(retained * retained, axis=-1, keepdims=True) + norm_eps)
            gate = g_v[h, at, :].astype(F32)
            gate = gate / (1.0 + jnp.exp(-gate))
            out = (gate * retained * scale * gain).astype(BF16)
            g_v[h, at, :] = out

            @pl.when((i != 0) if h < heads - 1 else ((i != 0) & (i != L - 1)))
            def _():
                head_copy(h, i).start()

            @pl.when(i == 0)
            def _():
                heads_v[:, pl.ds(pl.multiple_of(t * width + h * hd, hd), hd)] = out

        loop(L, piece)

    for k in order[-held:]:
        pass_on(k)
    for h in range(heads):
        finish(h)
        if h == 0:
            for k in order[2:5]:
                hand_over(k)
    for k in order[5:]:
        hand_over(k)

    done(x_v.at[0:chips], gc_r)
    load_weight(0).wait()
    load_weight(1).wait()
    hidden_width = hid.shape[1]
    tile = 256 if hidden_width % 256 == 0 else 128

    def up(n):
        at = pl.ds(pl.multiple_of(n * tile, tile), tile)
        x = x_v[...].reshape(L * group, D)
        both = dot(x, jnp.concatenate([wg_v[:, at], wu_v[:, at]], axis=1))
        gate, rise = both[:, :tile], both[:, tile:]
        hid[:, at] = (gate / (1.0 + jnp.exp(-gate)) * rise).astype(BF16)

    loop(hidden_width // tile, up)

    load_weight(2).wait()

    def share(n):
        done(rbuf.at[n], c2_r.at[n])
        for v in range(1, chips):
            yy = chip_ahead(v)
            total = ybuf[n, 2 * yy + c].astype(F32) + rbuf[n, yy].astype(F32)
            ysend[n, v - 1] = total.astype(BF16)
            chip_sum(n, v).start()

    def down(n):
        at = pl.ds(pl.multiple_of(n * COLS, COLS), COLS)
        ybuf[n] = dot(hid[...], wd_v[:, at]).astype(BF16).reshape(ybuf.shape[1:])
        for yy in range(chips):
            core_sum(n, yy).start()

        @pl.when(n > 0)
        def _():
            share(n - 1)

    loop(NT, down)
    share(NT - 1)
    last_copy().start()

    load_weight(3).wait()
    done(heads_v.at[:, 0 : (heads * (L - 1) - 1) * hd], h_r.at[0])
    heads_v[:, last_rows] = jnp.zeros_like(hlast)

    def parts(n):
        for i in range(2):
            at = (2 * n + i) * R
            rows_at = pl.ds(pl.multiple_of(lax.rem(at, BLOCK), R), R)
            yield at // BLOCK, rows_at, slice(i * hd, (i + 1) * hd)

    def project(n):
        at = pl.ds(pl.multiple_of(n * COLS, COLS), COLS)
        sums = dot(heads_v[...], wo_v[:, at])
        for plane, rows_at, cols in parts(n):
            local[plane, rows_at, :] = sums[:, cols]
        total = ybuf[n, t].astype(F32) + rbuf[n, y].astype(F32)
        done(yrecv.at[n], y2_r.at[n])
        for v in range(1, chips):
            total = total + yrecv[n, v - 1].astype(F32)
        fin[n] = total.astype(BF16).reshape(fin.shape[1:])
        for k in range(1, E):
            back(n, k).start()
        ret[n, e] = fin[n, e]

    loop(NT, project)

    weight = chosen * jnp.where(first, rw_ref[0:1, :], rw_ref[1:2, :])
    terms = split3(weight)
    for n in range(NT):
        done(ret.at[n, 0 : E - 1], r_r.at[n])
        got = ret[n].reshape(group, COLS)
        total = dot(terms[0], got, 0, 0) + dot(terms[1], got, 0, 0) + dot(terms[2], got, 0, 0)
        omoe[:, n * COLS : (n + 1) * COLS] = total.astype(BF16)

    last_copy().wait_recv()

    def project_last(n):
        at = pl.ds(pl.multiple_of(n * COLS, COLS), COLS)
        sums = dot(hlast[...], wo_v[last_rows, at])
        for plane, rows_at, cols in parts(n):
            to = pl.ds(pl.multiple_of(n * COLS + cols.start, hd), hd)
            obuf[:, to] = (local[plane, rows_at, :] + sums[:, cols]).astype(BF16)

    loop(NT, project_last)

    done(x_v.at[0, 0 : E - 1], a_s)
    done(x_v.at[0 : chips - 1], gy_s)
    done(x_v.at[0:chips], gc_s)
    done(drecv.at[0 : G - 1], d_s)

    @pl.when(upper_half == 0)
    def _():
        done(tsend, t_s)

    for h in range(heads):
        done(smsg.at[h, 0 : G - 1], s1_s.at[h])
        done(pout.at[h, 0 : G - 1], s2_s.at[h])
        done(heads_v.at[:, 0 : (L - 1) * hd], h_s.at[h])
    done(rbuf, c2_s)
    done(ysend, y2_s)
    for n in range(NT):
        done(fin.at[n, 0 : E - 1], r_s.at[n])


def on_device(
    mix_query, mix_key, mix_value, mix_gate, log_decay, ret_gain, w_out,
    moe_in, route_ids, route_weights, moe_gain, w_gate, w_up, w_down,
):
    E = lax.axis_size("ep")
    L = lax.axis_size("tp")
    chips = L // 2
    rows, width = mix_query.shape
    heads = width // HEAD_DIM
    blocks = rows // BLOCK
    steps = heads * blocks
    half = HEAD_DIM // 2
    tokens, D = moe_in.shape
    capacity = 4 * tokens // E
    group = E * capacity
    hidden = w_gate.shape[2]
    NT = D // COLS
    R = rows // L
    G = E // 2
    part = HEAD_DIM // G
    inverse = 10000.0 ** (-(np.arange(half) * 2.0) / HEAD_DIM)
    fine = np.arange(BLOCK)[:, None] * inverse[None, :]
    coarse = (np.arange(E * blocks) * BLOCK)[:, None, None] * inverse[None, None, :]
    tables = [np.asarray(f(x), np.float32) for x in (fine, coarse) for f in (np.cos, np.sin)]
    hbm = pl.BlockSpec(memory_space=pl.ANY)
    pad = -(-steps // 8) * 8
    V = pltpu.VMEM
    S = pltpu.SemaphoreType.DMA
    return pl.pallas_call(
        layer_kernel,
        in_specs=[hbm] * 18,
        out_specs=[pl.BlockSpec(memory_space=pltpu.VMEM)] * 2,
        out_shape=[
            pltpu.VMEM((R, D), BF16),
            pltpu.VMEM((tokens, D), BF16),
        ],
        scratch_shapes=[
            V((tokens, D), BF16), V((2, tokens), jnp.int32), V((2, tokens), F32),
            V((1, D), F32), V((1, width), F32), V((heads, rows), F32),
            V((BLOCK, half), F32), V((BLOCK, half), F32),
            V((E * blocks, 1, half), F32), V((E * blocks, 1, half), F32),
            V((heads, rows, HEAD_DIM), BF16), V((heads, rows, HEAD_DIM), BF16),
            V((heads, rows, HEAD_DIM), BF16), V((heads, rows, HEAD_DIM), BF16),
            V((D, hidden), BF16), V((D, hidden), BF16), V((hidden, D), BF16), V(w_out.shape, BF16),
            V((E, capacity, D), BF16), V((L, E, capacity, D), BF16), V((L * group, hidden), BF16),
            V((NT, L, group, COLS), BF16), V((NT, chips, group, COLS), BF16),
            V((NT, chips - 1, group, COLS), BF16), V((NT, chips - 1, group, COLS), BF16),
            V((NT, E, capacity, COLS), BF16), V((NT, E, capacity, COLS), BF16),
            V((pad, BLOCK), F32), V((pad, BLOCK), F32), V((pad, HEAD_DIM), F32),
            V((steps, BLOCK, HEAD_DIM), F32), V((HEAD_DIM, HEAD_DIM), F32),
            V((steps, HEAD_DIM, HEAD_DIM), F32),
            V((8, HEAD_DIM), F32), V((G, 8, HEAD_DIM), F32),
            V((heads, G, part, HEAD_DIM), BF16), V((heads, G, part, HEAD_DIM), BF16),
            V((heads, part, HEAD_DIM), BF16), V((heads, part, HEAD_DIM), BF16),
            V((heads, G, part, HEAD_DIM), BF16), V((heads, G, part, HEAD_DIM), BF16),
            V((R, D), BF16), V((R, HEAD_DIM), BF16),
            S((10,)), S((4, heads)), S((4,)), S(()), S((E,)),
            S(()), S((chips - 1, E)), S(()), S(()),
            S(()), S(()), S((heads,)), S((heads,)), S(()), S((heads,)), S((heads,)), S((heads,)),
            S((heads,)), S((2,)), S(()), S((NT,)), S(()), S((NT,)), S((NT,)), S((NT,)),
        ],
        compiler_params=pltpu.CompilerParams(
            collective_id=0, has_side_effects=True, vmem_limit_bytes=VMEM_LIMIT
        ),
        name="layer",
    )(
        moe_in, route_ids.T, route_weights.T, moe_gain.reshape(1, -1), ret_gain.reshape(1, -1),
        log_decay.T, *tables,
        mix_query, mix_key, mix_value, mix_gate, w_gate, w_up, w_down, w_out,
    )


def solution(mesh):
    in_specs = (
        P("ep", "tp"),
        P("ep", "tp"),
        P("ep", "tp"),
        P("ep", "tp"),
        P("ep", "tp"),
        P("tp"),
        P(),
        P(("ep", "tp"), None),
        P(("ep", "tp"), None),
        P(("ep", "tp"), None),
        P(),
        P("ep", None, "tp"),
        P("ep", None, "tp"),
        P("ep", "tp", None),
    )
    out_specs = (P(("ep", "tp"), None), P(("ep", "tp"), None))
    return jax.shard_map(
        lambda *args: tuple(on_device(*args)), mesh=mesh, in_specs=in_specs, out_specs=out_specs,
        check_vma=False,
    )
```

time: 82.4 us -> 65.5 us (0.79)
  Pallas kernels: 77.8 us -> 62.7 us
  local copies, waits for them, and re-layouts: 3.85 us -> 1.98 us
    pallas_call x1, Pallas kernels: 77.8 us -> 62.7 us  [on_device(): pl.pallas_call(layer_kernel, in_specs=[hbm] * 18, out_specs=[pl.BlockSpec...]
    unnamed x4 -> x2, local copies, waits for them, and re-layouts: 3.85 us -> 1.98 us
where the time goes in v1:
time: 65.5 us; the launch traced here: 65.3 us
  Pallas kernels  62.7 us (96%)
  local copies, waits for them, and re-layouts  1.98 us (3%)
    pallas_call x1, Pallas kernels, on_device(): pl.pallas_call(layer_kernel, in_specs=[hbm] * 18, out_specs=[pl.BlockSpec...  62.7 us
    unnamed x2, local copies, waits for them, and re-layouts  1.98 us

profile of v1, /device:TPU:0, one launch (start us, length us, event | category | flops | bytes accessed | tf_op | source)
XLA Modules:
  0.0 65.3 jit_solution(13368788638024979799)
XLA Ops:
  0.6 62.7 %layer.1 = (bf16[512,2048]{1,0:T(8,128)(2,1)S(1)}, bf16[32,2048]{1,0:T(8,128)(2,1)S(1)}) custom-call(bf16[32,2048]{1,0:T(8,128)(2,1)} %x_hbm.1, s32[2,32]{1,0:T(2,128)} %bitcast.8, f32[2,32]{1,0:T(2,128)} %bitcast.9, f32[1,2048]{1,0:T(1,128)} %bitcast.6, f32[1,512]{1,0:T(1,128)} %bitcast.7, f32[2,2048]{1,0:T(2,128)} %bitcast.5, ...), custom_call_target="tpu_custom_call" | custom-call | tf_op jit(solution)/shard_map/layer/pallas_call | solution.py:611
  63.4 1.3 %copy.22 = bf16[512,2048]{1,0:T(8,128)(2,1)} copy(bf16[512,2048]{1,0:T(8,128)(2,1)S(1)} %get-tuple-element.2) | data formatting | bytes 4194304
  64.7 0.7 %copy.23 = bf16[32,2048]{1,0:T(8,128)(2,1)} copy(bf16[32,2048]{1,0:T(8,128)(2,1)S(1)} %get-tuple-element.3) | data formatting | bytes 262144

commit v2 on v1

--- a/solution.py
+++ b/solution.py
@@ -30,12 +30,12 @@
     return a, b, c
 
 
-def loop(count, body):
+def loop(count, body, unroll=False):
     def step(i, carry):
         body(i)
         return carry
 
-    lax.fori_loop(0, count, step, 0)
+    lax.fori_loop(0, count, step, 0, unroll=unroll)
 
 
 def slots_of(ids, capacity, count):
@@ -328,7 +328,7 @@
                     def _():
                         pass_on(k)
 
-        loop(blocks, update)
+        loop(blocks, update, True)
         smsg[h] = state[...].astype(BF16).reshape(smsg.shape[1:])
         for k in range(1, G):
             scatter(h, k).start()
@@ -490,7 +490,7 @@
         gate, rise = both[:, :tile], both[:, tile:]
         hid[:, at] = (gate / (1.0 + jnp.exp(-gate)) * rise).astype(BF16)
 
-    loop(hidden_width // tile, up)
+    loop(hidden_width // tile, up, True)
 
     load_weight(2).wait()
 
@@ -559,7 +559,7 @@
             to = pl.ds(pl.multiple_of(n * COLS + cols.start, hd), hd)
             obuf[:, to] = (local[plane, rows_at, :] + sums[:, cols]).astype(BF16)
 
-    loop(NT, project_last)
+    loop(NT, project_last, True)
 
     done(x_v.at[0, 0 : E - 1], a_s)
     done(x_v.at[0 : chips - 1], gy_s)

time: 65.5 us -> 65.1 us (level)
  no operation moved by 1% of the time
where the time goes in v2:
time: 65.1 us; the launch traced here: 64.9 us
  Pallas kernels  62.3 us (96%)
  local copies, waits for them, and re-layouts  1.98 us (3%)
    pallas_call x1, Pallas kernels, on_device(): pl.pallas_call(layer_kernel, in_specs=[hbm] * 18, out_specs=[pl.BlockSpec...  62.3 us
    unnamed x2, local copies, waits for them, and re-layouts  1.98 us

profile of v2, /device:TPU:0, one launch (start us, length us, event | category | flops | bytes accessed | tf_op | source)
XLA Modules:
  0.0 64.9 jit_solution(17393626101410210497)
XLA Ops:
  0.6 62.3 %layer.1 = (bf16[512,2048]{1,0:T(8,128)(2,1)S(1)}, bf16[32,2048]{1,0:T(8,128)(2,1)S(1)}) custom-call(bf16[32,2048]{1,0:T(8,128)(2,1)} %x_hbm.1, s32[2,32]{1,0:T(2,128)} %bitcast.8, f32[2,32]{1,0:T(2,128)} %bitcast.9, f32[1,2048]{1,0:T(1,128)} %bitcast.6, f32[1,512]{1,0:T(1,128)} %bitcast.7, f32[2,2048]{1,0:T(2,128)} %bitcast.5, ...), custom_call_target="tpu_custom_call" | custom-call | tf_op jit(solution)/shard_map/layer/pallas_call | solution.py:611
  62.9 1.3 %copy.22 = bf16[512,2048]{1,0:T(8,128)(2,1)} copy(bf16[512,2048]{1,0:T(8,128)(2,1)S(1)} %get-tuple-element.2) | data formatting | bytes 4194304
  64.3 0.7 %copy.23 = bf16[32,2048]{1,0:T(8,128)(2,1)} copy(bf16[32,2048]{1,0:T(8,128)(2,1)S(1)} %get-tuple-element.3) | data formatting | bytes 262144
